TPU v7x, 32 devices: a whole 2x2x4 slice. The times are simulated.
32 devices in a mesh: grp: 2 (over x), ep: 16 (over z, y, core).
Axes of the slice: x: 2, y: 2, z: 4, core: 2. Of those that a mesh axis runs over, the one named last changes fastest.
Arguments:
- resid: bfloat16 [384, 2048], P(('grp', 'ep')), parts along dimension 0, may hold values from -6 to 6
- norm_gains: float32 [4, 2048], replicated, may hold values from 0.1 to 1.9
- w_query: bfloat16 [2048, 1024], P(None, 'ep'), may hold values from -0.125 to 0.125
- w_key: bfloat16 [2048, 1024], P(None, 'ep'), may hold values from -0.125 to 0.125
- w_value: bfloat16 [2048, 1024], P(None, 'ep'), may hold values from -0.125 to 0.125
- w_outgate: bfloat16 [2048, 1024], P(None, 'ep'), may hold values from -0.125 to 0.125
- w_igate: bfloat16 [2048, 8], replicated, may hold values from -0.125 to 0.125
- w_fgate: bfloat16 [2048, 8], replicated, may hold values from -0.125 to 0.125
- igate_bias: float32 [8], replicated, may hold values from -1 to 1
- fgate_bias: float32 [8], replicated, may hold values from -1 to 5
- state_matrix: float32 [384, 8, 128, 128], P(('grp', 'ep')), parts along dimension 0, may hold values from -0.8 to 0.8
- state_norm: float32 [384, 8, 128], P(('grp', 'ep')), parts along dimension 0, may hold values from -2.4 to 2.4
- state_max: float32 [384, 8], P(('grp', 'ep')), parts along dimension 0, may hold values from -1 to 1
- w_mix_out: bfloat16 [1024, 2048], replicated, may hold values from -0.1875 to 0.1875
- routes: int32 [384, 2], P(('grp', 'ep')), parts along dimension 0, may hold values from 0 to 15, all different within a row; in each aligned block of 12 rows (0 to 11, 12 to 23, ...) at most 2 rows name the same one
- route_scores: bfloat16 [384, 2], P(('grp', 'ep')), parts along dimension 0, may hold values from 0.099609375 to 1
- expert_gate: bfloat16 [16, 2048, 512], P('ep'), may hold values from -0.125 to 0.125
- expert_up: bfloat16 [16, 2048, 512], P('ep'), may hold values from -0.125 to 0.125
- expert_down: bfloat16 [16, 512, 2048], P('ep'), may hold values from -0.25 to 0.25
- dense_gate: bfloat16 [2048, 8192], P(None, 'ep'), may hold values from -0.125 to 0.125
- dense_up: bfloat16 [2048, 8192], P(None, 'ep'), may hold values from -0.125 to 0.125
- dense_down: bfloat16 [8192, 2048], P('ep'), may hold values from -0.0625 to 0.0625
- branch_weight: bfloat16 [2048], replicated, may hold values from -0.125 to 0.125
Outputs:
- out_stream: bfloat16 [384, 2048], P(('grp', 'ep')), parts along dimension 0
- new_matrix: float32 [384, 8, 128, 128], P(('grp', 'ep')), parts along dimension 0
- new_norm: float32 [384, 8, 128], P(('grp', 'ep')), parts along dimension 0
- new_max: float32 [384, 8], P(('grp', 'ep')), parts along dimension 0
There are 2 independent parts, one for each index of `grp`. A program takes and returns all parts, laid end to end along the dimension named above; an argument that names none is the same for every part. Nothing has to cross between parts.
Inputs may be any that keep to these rules, and one draw needn't show every extreme that they name: `routes`: each row names 2 different experts. In each aligned block of 12 rows (the rows of one device) no expert is named by more than 2 rows, a bound that some block reaches.
All inputs are finite; a program needn't handle non-finite values.
Results may differ from a plain program's by a relative error of at most 0.015.
Values may be sent and summed in bfloat16 or wider, within the bound.
A program may use at most 128 MiB of HBM per device.

v0:
```python
import jax
import jax.numpy as jnp
from jax import lax
from jax.sharding import PartitionSpec as P

CAP = 2


def rms_scale(values, gains):
    return values * lax.rsqrt(jnp.mean(values * values, axis=-1, keepdims=True) + 1e-06) * gains


def expert_batch(picked, gate_matrix, up_matrix, down_matrix):
    gate_out = jnp.einsum("jrd,jdf->jrf", picked, gate_matrix, preferred_element_type=jnp.float32)
    up_out = jnp.einsum("jrd,jdf->jrf", picked, up_matrix, preferred_element_type=jnp.float32)
    hidden = (jax.nn.silu(gate_out) * up_out).astype(jnp.bfloat16)
    return jnp.einsum(
        "jrf,jfd->jrd", hidden, down_matrix, preferred_element_type=jnp.float32
    ).astype(jnp.bfloat16)


def route_tables(routes, route_scores, expert_ids):
    onehot = (routes[:, :, None] == expert_ids[None, None, :]).astype(jnp.float32)
    scores = route_scores.astype(jnp.float32)
    shares = scores / jnp.sum(scores, axis=-1, keepdims=True)
    weights = jnp.sum(shares[:, :, None] * onehot, axis=1)
    hit_count = jnp.sum(onehot, axis=1)
    return (weights, hit_count)


def exchanged_experts(
    branch_in, routes, route_scores, expert_gate, expert_up, expert_down, devices_ep
):
    experts = expert_gate.shape[0] * devices_ep
    weights, hit_count = route_tables(routes, route_scores, jnp.arange(experts, dtype=jnp.int32))
    hit_int = hit_count.astype(jnp.int32)
    rank_index = jnp.cumsum(hit_int, axis=0) - hit_int
    slot_range = jnp.arange(CAP, dtype=jnp.int32)
    chosen = (
        (rank_index.T[:, None, :] == slot_range[None, :, None]) & (hit_count.T[:, None, :] > 0.5)
    ).astype(jnp.float32)
    outgoing = jnp.einsum(
        "ect,td->ecd", chosen.astype(jnp.bfloat16), branch_in, preferred_element_type=jnp.float32
    ).astype(jnp.bfloat16)
    incoming = lax.all_to_all(outgoing, "ep", split_axis=0, concat_axis=1, tiled=True)
    produced = expert_batch(incoming, expert_gate, expert_up, expert_down)
    returned = lax.all_to_all(produced, "ep", split_axis=1, concat_axis=0, tiled=True)
    weighted = chosen * weights.T[:, None, :]
    each_expert = jnp.einsum(
        "ect,ecd->etd", weighted, returned.astype(jnp.float32), precision=lax.Precision.HIGHEST
    )
    return jnp.sum(each_expert.astype(jnp.bfloat16).astype(jnp.float32), axis=0)


def local(
    resid,
    norm_gains,
    w_query,
    w_key,
    w_value,
    w_outgate,
    w_igate,
    w_fgate,
    igate_bias,
    fgate_bias,
    state_matrix,
    state_norm,
    state_max,
    w_mix_out,
    routes,
    route_scores,
    expert_gate,
    expert_up,
    expert_down,
    dense_gate,
    dense_up,
    dense_down,
    branch_weight,
):
    seqs_local = resid.shape[0]
    heads = state_matrix.shape[1]
    head_size = state_matrix.shape[2]
    devices_ep = lax.axis_size("ep")
    resid32 = resid.astype(jnp.float32)
    normed = rms_scale(resid32, norm_gains[0]).astype(jnp.bfloat16)
    row_piece = lax.all_gather(normed, "ep", axis=0, tiled=True)
    projected = jnp.stack(
        [
            jnp.dot(row_piece, matrix, preferred_element_type=jnp.float32).astype(jnp.bfloat16)
            for matrix in (w_query, w_key, w_value, w_outgate)
        ],
        axis=1,
    )
    own_proj = lax.all_to_all(projected, "ep", split_axis=0, concat_axis=2, tiled=True)
    head_shape = (seqs_local, heads, head_size)
    query = own_proj[:, 0].astype(jnp.float32).reshape(head_shape)
    key_heads = own_proj[:, 1].astype(jnp.float32).reshape(head_shape) * head_size ** (-0.5)
    value_heads = own_proj[:, 2].astype(jnp.float32).reshape(head_shape)
    outgate = own_proj[:, 3].astype(jnp.float32).reshape(head_shape)
    ipre = jnp.dot(normed, w_igate, preferred_element_type=jnp.float32) + igate_bias
    fpre = jnp.dot(normed, w_fgate, preferred_element_type=jnp.float32) + fgate_bias
    logf = jax.nn.log_sigmoid(fpre)
    new_max = jnp.maximum(ipre, logf + state_max)
    keep_gain = jnp.exp(logf + state_max - new_max)
    write_gain = jnp.exp(ipre - new_max)
    new_matrix = (
        keep_gain[:, :, None, None] * state_matrix
        + write_gain[:, :, None, None] * value_heads[:, :, :, None] * key_heads[:, :, None, :]
    )
    new_norm = keep_gain[:, :, None] * state_norm + write_gain[:, :, None] * key_heads
    numer = jnp.einsum("shed,shd->she", new_matrix, query, precision=lax.Precision.HIGHEST)
    denom = jnp.sum(new_norm * query, axis=-1)
    cell = numer / jnp.maximum(jnp.abs(denom), 1.0)[:, :, None]
    gated = (
        (jax.nn.sigmoid(outgate) * cell).reshape(seqs_local, heads * head_size).astype(jnp.bfloat16)
    )
    mixed = jnp.dot(gated, w_mix_out, preferred_element_type=jnp.float32)
    middle = resid32 + rms_scale(mixed, norm_gains[1])
    branch_in = rms_scale(middle, norm_gains[2]).astype(jnp.bfloat16)
    all_rows = lax.all_gather(branch_in, "ep", axis=0, tiled=True)
    moe_own = exchanged_experts(
        branch_in, routes, route_scores, expert_gate, expert_up, expert_down, devices_ep
    )
    gate_out = jnp.dot(all_rows, dense_gate, preferred_element_type=jnp.float32)
    up_out = jnp.dot(all_rows, dense_up, preferred_element_type=jnp.float32)
    hidden = (jax.nn.silu(gate_out) * up_out).astype(jnp.bfloat16)
    logit = jnp.dot(all_rows, branch_weight, preferred_element_type=jnp.float32)
    summed = lax.psum_scatter(
        (
            jnp.dot(hidden, dense_down, preferred_element_type=jnp.float32)
            * jax.nn.sigmoid(logit)[:, None]
        ).astype(jnp.bfloat16),
        "ep",
        scatter_dimension=0,
        tiled=True,
    ).astype(jnp.float32)
    combined = moe_own + summed
    out_stream = (middle + rms_scale(combined, norm_gains[3])).astype(jnp.bfloat16)
    return (out_stream, new_matrix, new_norm, new_max)


def solution(mesh):
    placed = (
        P(("grp", "ep"), None),
        P(),
        P(None, "ep"),
        P(None, "ep"),
        P(None, "ep"),
        P(None, "ep"),
        P(),
        P(),
        P(),
        P(),
        P(("grp", "ep"), None, None, None),
        P(("grp", "ep"), None, None),
        P(("grp", "ep"), None),
        P(),
        P(("grp", "ep"), None),
        P(("grp", "ep"), None),
        P("ep", None, None),
        P("ep", None, None),
        P("ep", None, None),
        P(None, "ep"),
        P(None, "ep"),
        P("ep", None),
        P(),
    )
    return jax.shard_map(
        local,
        mesh=mesh,
        in_specs=placed,
        out_specs=(
            P(("grp", "ep"), None),
            P(("grp", "ep"), None, None, None),
            P(("grp", "ep"), None, None),
            P(("grp", "ep"), None),
        ),
        check_vma=False,
    )
```

profile of v0, /device:TPU:0, one launch (start us, length us, event | category | flops | bytes accessed | tf_op | source)
XLA Modules:
  0.0 160.2 jit_solution(14762901746730829710)
XLA Ops:
  0.7 1.0 fusion.62
  1.7 1.0 fusion.30
  2.6 1.0 fusion.61
  3.6 27.6 %all-gather = bf16[16,12,2048]{2,1,0:T(8,128)(2,1)} all-gather(bf16[1,12,2048]{2,1,0:T(8,128)(2,1)S(1)} %fusion.61), channel_id=1, replica_groups=mesh['grp'=2,'ep'=16] {'ep'}, dimensions={0}, use_global_device_ids=true | all-gather | bytes 835584 | tf_op jit(solution)/shard_map/all_gather | solution.py:86
  31.2 1.3 reshape.139
  32.5 0.4 fusion.17
  33.0 0.4 fusion.18
  33.5 0.4 fusion.19
  33.9 0.4 fusion.20
  34.5 0.8 reshape.151
  35.3 3.5 %all-to-all-start = ((bf16[16,2,1536]{2,1,0:T(2,128)(2,1)}), bf16[16,2,1536]{2,1,0:T(2,128)(2,1)S(1)}, u32[]{:S(2)}, u32[]{:S(2)}) async-start(bf16[16,2,1536]{2,1,0:T(2,128)(2,1)} %reshape.151), calls=%async_computation | async-start | bytes 196608 | tf_op jit(solution)/shard_map/all_to_all | solution.py:94
  39.2 0.2 fusion.54
  39.5 0.2 broadcast_multiply_fusion.2
  40.2 5.9 %all-to-all-done = bf16[16,2,1536]{2,1,0:T(2,128)(2,1)S(1)} async-done(((bf16[16,2,1536]{2,1,0:T(2,128)(2,1)}), bf16[16,2,1536]{2,1,0:T(2,128)(2,1)S(1)}, u32[]{:S(2)}, u32[]{:S(2)}) %all-to-all-start) | async-done | bytes 98336 | tf_op jit(solution)/shard_map/all_to_all | solution.py:94
  46.4 0.2 all_to_all.32
  46.6 0.2 slice_reduce_fusion
  46.9 0.7 multiply_reduce_fusion.3
  47.6 4.5 %multiply_add_fusion = f32[12,8,128,128]{3,2,1,0:T(8,128)S(1)} fusion(f32[12,8,128,128]{3,2,1,0:T(8,128)} %param.33, f32[12,8,128]{2,1,0:T(8,128)S(1)} %get-tuple-element.14, f32[12,8,128]{2,1,0:T(8,128)S(1)} %get-tuple-element.21, f32[12,8]{1,0:T(8,128)S(1)} %copy.78), kind=kLoop, calls=%fused_computation | loop fusion | flops 4718592 | bytes 12681600 | tf_op jit(solution)/shard_map/add | solution.py:107
  52.2 5.0 %fusion.43 = f32[12,8,1,128]{3,2,1,0:T(1,128)S(1)} fusion(f32[12,8,128,128]{3,2,1,0:T(8,128)S(1)} %multiply_add_fusion, bf16[12,4,1024]{2,1,0:T(4,128)(2,1)S(1)} %all_to_all.32), kind=kOutput, calls=%fused_computation.61 | convolution fusion | flops 18874368 | bytes 6389760 | tf_op jit(solution)/shard_map/shed,shd->she/dot_general | solution.py:111
  57.3 0.8 multiply_reduce_fusion.2
  58.1 0.2 multiply_reduce_fusion.1
  58.4 22.2 %all-gather.1 = bf16[16,12,2048]{2,1,0:T(8,128)(2,1)} all-gather(bf16[1,12,2048]{2,1,0:T(8,128)(2,1)S(1)} %fusion.58), channel_id=1, replica_groups=mesh['grp'=2,'ep'=16] {'ep'}, dimensions={0}, use_global_device_ids=true | all-gather | bytes 835584 | tf_op jit(solution)/shard_map/all_gather | solution.py:120
  80.6 1.3 reshape.141
  81.9 2.9 %fusion.63 = f32[192,512]{1,0:T(8,128)} fusion(bf16[192,2048]{1,0:T(8,128)(2,1)S(1)} %reshape.141, bf16[2048,512]{1,0:T(8,128)(2,1)} %param.42), kind=kOutput, calls=%fused_computation.106 | convolution fusion | flops 402653184 | bytes 3276800 | tf_op jit(solution)/shard_map/dot_general | solution.py:124
  84.8 0.3 fusion.64
  85.1 0.3 convolution_convert_fusion.2
  85.4 0.8 copy.88
  86.2 3.7 %all-to-all-start.1 = ((bf16[16,2,2048]{2,1,0:T(2,128)(2,1)}), bf16[16,2,2048]{2,1,0:T(2,128)(2,1)S(1)}, u32[]{:S(2)}, u32[]{:S(2)}) async-start(bf16[16,2,2048]{2,1,0:T(2,128)(2,1)} %copy.88), calls=%async_computation.1 | async-start | bytes 262144 | tf_op jit(solution)/shard_map/all_to_all | solution.py:45
  89.9 3.6 %fusion.2 = bf16[192,2048]{1,0:T(8,128)(2,1)} fusion(bf16[512,2048]{1,0:T(8,128)(2,1)S(1)} %copy-done, bf16[192,2048]{1,0:T(8,128)(2,1)S(1)} %reshape.141, bf16[2048,512]{1,0:T(8,128)(2,1)} %param.43, f32[192]{0:T(256)S(1)} %add_divide_fusion, f32[192,512]{1,0:T(8,128)} %fusion.63), kind=kOutput, calls=%fused_computation.4 | convolution fusion | flops 806682624 | bytes 6161152 | tf_op jit(solution)/shard_map/dot_general | solution.py:130
  93.5 4.1 %all-to-all-done.1 = bf16[16,2,2048]{2,1,0:T(2,128)(2,1)S(1)} async-done(((bf16[16,2,2048]{2,1,0:T(2,128)(2,1)}), bf16[16,2,2048]{2,1,0:T(2,128)(2,1)S(1)}, u32[]{:S(2)}, u32[]{:S(2)}) %all-to-all-start.1) | async-done | bytes 131104 | tf_op jit(solution)/shard_map/all_to_all | solution.py:45
  97.6 2.0 %fusion.7 = f32[32,512]{1,0:T(8,128)S(1)} fusion(bf16[32,2048]{1,0:T(8,128)(2,1)S(1)} %reshape.130, bf16[1,2048,512]{2,1,0:T(8,128)(2,1)} %param.39), kind=kOutput, calls=%fused_computation.11 | convolution fusion | flops 67108864 | bytes 2293760 | tf_op jit(solution)/shard_map/jrd,jdf->jrf/dot_general | solution.py:14
  99.7 3.2 %fusion.3 = bf16[1,32,2048]{2,1,0:T(8,128)(2,1)S(1)} fusion(bf16[1,512,2048]{2,1,0:T(8,128)(2,1)} %param.41, bf16[32,2048]{1,0:T(8,128)(2,1)S(1)} %reshape.130, bf16[1,2048,512]{2,1,0:T(8,128)(2,1)} %param.40, f32[32,512]{1,0:T(8,128)S(1)} %fusion.7), kind=kOutput, calls=%fused_computation.7 | convolution fusion | flops 134381568 | bytes 4521984 | tf_op jit(solution)/shard_map/jrf,jfd->jrd/dot_general | solution.py:17
  102.9 0.2 copy.98
  103.1 0.5 broadcast.129
  103.6 1.4 reduce.4
  105.0 0.8 reshape.153
  105.8 3.5 %all-to-all-start.2 = ((bf16[16,2,2048]{2,1,0:T(2,128)(2,1)}), bf16[16,2,2048]{2,1,0:T(2,128)(2,1)S(1)}, u32[]{:S(2)}, u32[]{:S(2)}) async-start(bf16[16,2,2048]{2,1,0:T(2,128)(2,1)} %reshape.153), calls=%async_computation.2 | async-start | bytes 262144 | tf_op jit(solution)/shard_map/all_to_all | solution.py:47
  109.3 40.1 %fusion = bf16[16,2048]{1,0:T(8,128)(2,1)S(1)} fusion(bf16[192,2048]{1,0:T(8,128)(2,1)S(1)} %copy-done.4), kind=kCustom, calls=%all-reduce-scatter | all-reduce-scatter fusion | flops 524289 | bytes 852480
  149.4 1.3 collective-permute-start
  150.7 1.3 collective-permute-start.1
  152.0 1.3 collective-permute-start.2
  153.3 1.3 collective-permute-start.3
  154.7 0.6 dynamic-slice.4
  156.0 0.6 collective-permute-done.3
  156.5 0.7 concatenate
  157.4 0.7 bitcast_reduce_fusion
  158.3 1.1 fusion.9
  159.5 0.7 add_convert_fusion
  (83 shorter events, 2.4 us)
Async XLA Ops:
  0.6 89.3 %copy-start = (bf16[512,2048]{1,0:T(8,128)(2,1)S(1)}, bf16[512,2048]{1,0:T(8,128)(2,1)}, u32[]{:S(2)}) copy-start(bf16[512,2048]{1,0:T(8,128)(2,1)} %param.44) | copy-start | bytes 6291460
  0.6 31.8 %copy-start.5 = (bf16[2048,64]{0,1:T(8,128)(2,1)S(1)}, bf16[2048,64]{0,1:T(8,128)(2,1)}, u32[]{:S(2)}) copy-start(bf16[2048,64]{0,1:T(8,128)(2,1)} %param.25) | copy-start | bytes 786436
  2.6 30.3 %copy-start.6 = (bf16[2048,64]{0,1:T(8,128)(2,1)S(1)}, bf16[2048,64]{0,1:T(8,128)(2,1)}, u32[]{:S(2)}) copy-start(bf16[2048,64]{0,1:T(8,128)(2,1)} %param.26) | copy-start | bytes 786436
  32.5 1.0 copy-start.7
  32.5 1.3 copy-start.8
  32.9 5.9 %copy-start.14 = (bf16[12,2]{0,1:T(2,128)(2,1)S(1)}, bf16[12,2]{0,1:T(2,128)(2,1)}, u32[]{:S(2)}) copy-start(bf16[12,2]{0,1:T(2,128)(2,1)} %param.38) | copy-start | bytes 148
  32.9 6.0 %copy-start.12 = (s32[12,2]{0,1:T(2,128)S(1)}, s32[12,2]{0,1:T(2,128)}, u32[]{:S(2)}) copy-start(s32[12,2]{0,1:T(2,128)} %param.37) | copy-start | bytes 292
  32.9 6.2 %copy-start.3 = (bf16[12,2048]{1,0:T(8,128)(2,1)S(1)}, bf16[12,2048]{1,0:T(8,128)(2,1)}, u32[]{:S(2)}) copy-start(bf16[12,2048]{1,0:T(8,128)(2,1)} %param.23) | copy-start | bytes 147460
  32.9 6.2 %copy-start.15 = (bf16[2048,8]{0,1:T(8,128)(2,1)S(1)}, bf16[2048,8]{0,1:T(8,128)(2,1)}, u32[]{:S(2)}) copy-start(bf16[2048,8]{0,1:T(8,128)(2,1)} %param.30) | copy-start | bytes 98308
  33.0 6.2 %copy-start.17 = (f32[12,8]{0,1:T(8,128)S(1)}, f32[12,8]{0,1:T(8,128)}, u32[]{:S(2)}) copy-start(f32[12,8]{0,1:T(8,128)} %param.35) | copy-start | bytes 1156
  33.0 6.2 %copy-start.18 = (f32[8]{0:T(128)S(1)}, f32[8]{0:T(128)}, u32[]{:S(2)}) copy-start(f32[8]{0:T(128)} %param.32) | copy-start | bytes 100
  33.0 6.5 %copy-start.16 = (bf16[2048,8]{0,1:T(8,128)(2,1)S(1)}, bf16[2048,8]{0,1:T(8,128)(2,1)}, u32[]{:S(2)}) copy-start(bf16[2048,8]{0,1:T(8,128)(2,1)} %param.29) | copy-start | bytes 98308
  33.0 6.5 %copy-start.19 = (f32[8]{0:T(128)S(1)}, f32[8]{0:T(128)}, u32[]{:S(2)}) copy-start(f32[8]{0:T(128)} %param.31) | copy-start | bytes 100
  33.5 6.5 %copy-start.10 = (bf16[2048]{0:T(1024)(128)(2,1)S(1)}, bf16[2048]{0:T(1024)(128)(2,1)}, u32[]{:S(2)}) copy-start(bf16[2048]{0:T(1024)(128)(2,1)} %param.45) | copy-start | bytes 12292
  33.9 13.0 %copy-start.9 = (f32[12,8,128]{2,1,0:T(8,128)S(1)}, f32[12,8,128]{2,1,0:T(8,128)}, u32[]{:S(2)}) copy-start(f32[12,8,128]{2,1,0:T(8,128)} %param.34) | copy-start | bytes 147460
  35.3 10.9 %all-to-all-start = ((bf16[16,2,1536]{2,1,0:T(2,128)(2,1)}), bf16[16,2,1536]{2,1,0:T(2,128)(2,1)S(1)}, u32[]{:S(2)}, u32[]{:S(2)}) async-start(bf16[16,2,1536]{2,1,0:T(2,128)(2,1)} %reshape.151), calls=%async_computation | async-start | bytes 196608 | tf_op jit(solution)/shard_map/all_to_all | solution.py:94
  39.7 12.4 %copy-start.11 = (f32[12,8]{0,1:T(8,128)}, f32[12,8]{0,1:T(8,128)S(1)}, u32[]{:S(2)}) copy-start(f32[12,8]{0,1:T(8,128)S(1)} %get-tuple-element.10) | copy-start | bytes 1156
  52.1 5.0 %copy-start.1 = (f32[12,8,128,128]{3,2,1,0:T(8,128)}, f32[12,8,128,128]{3,2,1,0:T(8,128)S(1)}, u32[]{:S(2)}) copy-start(f32[12,8,128,128]{3,2,1,0:T(8,128)S(1)} %multiply_add_fusion) | copy-start | bytes 18874372
  52.1 5.1 %copy-start.2 = (bf16[1024,2048]{1,0:T(8,128)(2,1)S(1)}, bf16[1024,2048]{1,0:T(8,128)(2,1)}, u32[]{:S(2)}) copy-start(bf16[1024,2048]{1,0:T(8,128)(2,1)} %param.36) | copy-start | bytes 12582916
  86.2 11.4 %all-to-all-start.1 = ((bf16[16,2,2048]{2,1,0:T(2,128)(2,1)}), bf16[16,2,2048]{2,1,0:T(2,128)(2,1)S(1)}, u32[]{:S(2)}, u32[]{:S(2)}) async-start(bf16[16,2,2048]{2,1,0:T(2,128)(2,1)} %copy.88), calls=%async_computation.1 | async-start | bytes 262144 | tf_op jit(solution)/shard_map/all_to_all | solution.py:45
  99.7 9.6 %copy-start.4 = (bf16[192,2048]{1,0:T(8,128)(2,1)S(1)}, bf16[192,2048]{1,0:T(8,128)(2,1)}, u32[]{:S(2)}) copy-start(bf16[192,2048]{1,0:T(8,128)(2,1)} %fusion.2) | copy-start | bytes 2359300
  102.9 51.8 %copy-start.13 = (u32[32]{0:T(128)S(1)}, u32[32]{0:T(128)}, u32[]{:S(2)}) copy-start(u32[32]{0:T(128)} %constant.42) | copy-start | bytes 388
  105.8 51.5 %all-to-all-start.2 = ((bf16[16,2,2048]{2,1,0:T(2,128)(2,1)}), bf16[16,2,2048]{2,1,0:T(2,128)(2,1)S(1)}, u32[]{:S(2)}, u32[]{:S(2)}) async-start(bf16[16,2,2048]{2,1,0:T(2,128)(2,1)} %reshape.153), calls=%async_computation.2 | async-start | bytes 262144 | tf_op jit(solution)/shard_map/all_to_all | solution.py:47
  149.4 7.1 %collective-permute-start = (bf16[16,2048]{1,0:T(8,128)(2,1)S(1)}, bf16[16,2048]{1,0:T(8,128)(2,1)S(1)}, u32[]{:S(2)}, u32[]{:S(2)}) collective-permute-start(bf16[16,2048]{1,0:T(8,128)(2,1)S(1)} %fusion), channel_id=1, source_target_pairs={{0,1},{1,2},{2,3},{3,4},{4,5},{5,6},{6,7},{7,8},{8,9},{9,10},{10,1... | collective-permute-start | bytes 196616
  150.7 5.8 %collective-permute-start.1 = (bf16[16,2048]{1,0:T(8,128)(2,1)S(1)}, bf16[16,2048]{1,0:T(8,128)(2,1)S(1)}, u32[]{:S(2)}, u32[]{:S(2)}) collective-permute-start(bf16[16,2048]{1,0:T(8,128)(2,1)S(1)} %fusion), channel_id=1, source_target_pairs={{0,2},{1,3},{2,4},{3,5},{4,6},{5,7},{6,8},{7,9},{8,10},{9,11},{10,... | collective-permute-start | bytes 196616
  152.0 4.5 %collective-permute-start.2 = (bf16[16,2048]{1,0:T(8,128)(2,1)S(1)}, bf16[16,2048]{1,0:T(8,128)(2,1)S(1)}, u32[]{:S(2)}, u32[]{:S(2)}) collective-permute-start(bf16[16,2048]{1,0:T(8,128)(2,1)S(1)} %fusion), channel_id=1, source_target_pairs={{0,3},{1,4},{2,5},{3,6},{4,7},{5,8},{6,9},{7,10},{8,11},{9,12},{10... | collective-permute-start | bytes 196616
  153.3 3.2 %collective-permute-start.3 = (bf16[12,2048]{1,0:T(8,128)(2,1)S(1)}, bf16[12,2048]{1,0:T(8,128)(2,1)S(1)}, u32[]{:S(2)}, u32[]{:S(2)}) collective-permute-start(bf16[12,2048]{1,0:T(8,128)(2,1)S(1)} %slice.36), channel_id=1, source_target_pairs={{0,4},{1,5},{2,6},{3,7},{4,8},{5,9},{6,10},{7,11},{8,12},{9,13},{1... | collective-permute-start | bytes 147464
where the time goes:
time: 162 us; the launch traced here: 160 us
  blocking collectives  89.8 us (55%)
  matrix products  21.1 us (13%)
  starting transfers between devices  15.9 us (10%)
  waiting for transfers between devices  10.6 us (7%)
  local copies, waits for them, and re-layouts  10.5 us (6%)
  other arithmetic  10.4 us (6%)
  between operations  1.87 us (1%)
    unnamed x1, blocking collectives  40.1 us
    all_gather x1, blocking collectives, local(): row_piece = lax.all_gather(normed, 'ep', axis=0, tiled=True)  27.6 us
    all_gather x1, blocking collectives, local(): all_rows = lax.all_gather(branch_in, 'ep', axis=0, tiled=True)  22.2 us
    unnamed x55, local copies, waits for them, and re-layouts  6.65 us
    all_to_all x1, waiting for transfers between devices, local(): lax.all_to_all(projected, 'ep', split_axis=0, concat_axis=2, tiled=True)  5.94 us
    unnamed x4, starting transfers between devices  5.17 us
    dot_general x1, matrix products, local(): jnp.einsum('shed,shd->she', new_matrix, query, precision=lax.Precision.HI...  4.97 us
    add x1, other arithmetic, local(): keep_gain[:, :, None, None] * state_matrix  4.49 us
  transfers between devices with their start and end apart: 7, of which 3 were waited for; matrix products, arithmetic and copies ran while one was open for 29% of the time, Pallas kernels for 0%

commit v1 on v0

v1 whole, which is shorter than its diff:
```python
import functools

import jax
import jax.numpy as jnp
from jax import lax
from jax.experimental import pallas as pl
from jax.experimental.pallas import tpu as pltpu
from jax.sharding import PartitionSpec as P

MESH = pl.DeviceIdType.MESH
F32 = jnp.float32
BF16 = jnp.bfloat16
ROWS = 16
TABLE = 128
CHUNKS = 4


def rms_scale(values, gains):
    return values * lax.rsqrt(jnp.mean(values * values, axis=-1, keepdims=True) + 1e-06) * gains


def place():
    me = lax.axis_index("ep")
    return lax.div(me, 4), lax.rem(lax.div(me, 2), 2), lax.rem(me, 2)


def device(a, b, c):
    return {"ep": (a * 2 + b) * 2 + c}


def near_first(count):
    return sorted(range(1, count), key=lambda k: (min(k, count - k), k))


def push(src, dst, send_sem, recv_sem, to):
    copy = pltpu.make_async_remote_copy(
        src_ref=src, dst_ref=dst, send_sem=send_sem, recv_sem=recv_sem,
        device_id=to, device_id_type=MESH,
    )
    copy.start()
    return copy


def arrived(dst, send_sem, recv_sem, to):
    pltpu.make_async_remote_copy(
        src_ref=dst, dst_ref=dst, send_sem=send_sem, recv_sem=recv_sem,
        device_id=to, device_id_type=MESH,
    ).wait_recv()


def gather(buf, a, b, c, groups, send_z, send_y, send_d, recv):
    order = near_first(groups)
    y_peer, d_peer = device(a, 1 - b, c), device(a, b, 1 - c)
    sent = []

    def send(bb, aa, to, sem):
        block = buf.at[c, bb, aa]
        sent.append(push(block, block, sem, recv.at[c, bb, aa], to))

    def wait(cc, bb, aa):
        arrived(buf.at[cc, bb, aa], send_d.at[0, 0], recv.at[cc, bb, aa], d_peer)

    for k in order:
        send(b, a, device(lax.rem(a + k, groups), b, c), send_z.at[k])
    send(b, a, y_peer, send_y.at[0])
    send(b, a, d_peer, send_d.at[0, 0])
    for k in order:
        src = lax.rem(a + k, groups)
        wait(c, b, src)
        send(b, src, y_peer, send_y.at[k])
        send(b, src, d_peer, send_d.at[0, k])
    for k in [0] + order:
        src = lax.rem(a + k, groups)
        wait(c, 1 - b, src)
        send(1 - b, src, d_peer, send_d.at[1, k])
    for bb in range(2):
        for aa in range(groups):
            wait(1 - c, bb, aa)
    for copy in sent:
        copy.wait_send()


def project_kernel(
    n, resid_ref, gain_ref, wq_ref, wk_ref, wv_ref, wo_ref, out_ref,
    rows, local, landed, send_z, send_y, send_d, recv, send_x, recv_x,
):
    groups = n // 4
    a, b, c = place()
    me = lax.axis_index("ep")
    rows_local = resid_ref.shape[0]
    width = wq_ref.shape[1]
    barrier = pltpu.get_barrier_semaphore()
    for k in range(1, n):
        pl.semaphore_signal(
            barrier, inc=1, device_id={"ep": lax.rem(me + k, n)}, device_id_type=MESH
        )
    normed = rms_scale(resid_ref[...].astype(F32), gain_ref[...]).astype(BF16)
    rows[c, b, a] = jnp.zeros(rows.shape[3:], BF16)
    rows[c, b, a, 0:rows_local, :] = normed
    pl.semaphore_wait(barrier, n - 1)
    gather(rows, a, b, c, groups, send_z, send_y, send_d, recv)
    everything = rows[...].reshape(n * ROWS, rows.shape[-1])
    for m, w_ref in enumerate((wq_ref, wk_ref, wv_ref, wo_ref)):
        piece = jnp.dot(everything, w_ref[...], preferred_element_type=F32).astype(BF16)
        local[:, :, :, :, m * width : (m + 1) * width] = piece.reshape(2, 2, groups, ROWS, width)
    sent = []
    for k in range(1, n):
        to = lax.rem(me + k, n)
        block = local.at[lax.rem(to, 2), lax.rem(lax.div(to, 2), 2), lax.div(to, 4)]
        sent.append(push(block, landed.at[c, b, a], send_x.at[k], recv_x.at[c, b, a], {"ep": to}))
    landed[c, b, a] = local[c, b, a]
    for k in range(1, n):
        src = lax.rem(me + k, n)
        cc, bb, aa = lax.rem(src, 2), lax.rem(lax.div(src, 2), 2), lax.div(src, 4)
        arrived(landed.at[cc, bb, aa], send_x.at[k], recv_x.at[cc, bb, aa], {"ep": src})
    for aa in range(groups):
        for bb in range(2):
            for cc in range(2):
                start = ((aa * 2 + bb) * 2 + cc) * width
                for m in range(4):
                    out_ref[m, :, start : start + width] = landed[
                        cc, bb, aa, :, m * width : (m + 1) * width
                    ]
    for copy in sent:
        copy.wait_send()


def project(resid, gain, weights, n):
    rows_local, d = resid.shape
    width = weights[0].shape[1]
    groups = n // 4
    vmem = pl.BlockSpec(memory_space=pltpu.VMEM)
    return pl.pallas_call(
        functools.partial(project_kernel, n),
        out_shape=jax.ShapeDtypeStruct((4, ROWS, n * width), BF16),
        in_specs=[vmem] * 6,
        out_specs=vmem,
        scratch_shapes=[
            pltpu.VMEM((2, 2, groups, ROWS, d), BF16),
            pltpu.VMEM((2, 2, groups, ROWS, 4 * width), BF16),
            pltpu.VMEM((2, 2, groups, ROWS, 4 * width), BF16),
            pltpu.SemaphoreType.DMA((groups,)),
            pltpu.SemaphoreType.DMA((groups,)),
            pltpu.SemaphoreType.DMA((2, groups)),
            pltpu.SemaphoreType.DMA((2, 2, groups)),
            pltpu.SemaphoreType.DMA((n,)),
            pltpu.SemaphoreType.DMA((2, 2, groups)),
        ],
        compiler_params=pltpu.CompilerParams(
            collective_id=0, has_side_effects=True, vmem_limit_bytes=32 * 2**20
        ),
        name="project",
    )(resid, gain, *weights)


def branch_kernel(
    n, branch_ref, table_ref, middle_ref, gain_ref, gate_w_ref,
    eg_hbm, eu_hbm, ed_hbm, dg_hbm, du_hbm, dd_hbm, out_ref,
    rows, eg, eu, ed, dg, du, dd, hid_e, hid_d,
    term, recv1, part1, recv2, part2, recv3,
    load, send_z, send_y, send_d, recv, s1, r1, s2, r2, s3, r3,
):
    groups = n // 4
    a, b, c = place()
    me = lax.axis_index("ep")
    rows_local, d = branch_ref.shape
    experts_local = eg.shape[0]
    order = near_first(groups)
    y_peer, d_peer = device(a, 1 - b, c), device(a, b, 1 - c)
    barrier = pltpu.get_barrier_semaphore()
    for to in [device(lax.rem(a + k, groups), b, c) for k in order] + [y_peer, d_peer]:
        pl.semaphore_signal(barrier, inc=1, device_id=to, device_id_type=MESH)
    loads = []
    for i, (src, dst) in enumerate(
        ((dg_hbm, dg), (du_hbm, du), (eg_hbm, eg), (eu_hbm, eu), (dd_hbm, dd), (ed_hbm, ed))
    ):
        loads.append(pltpu.make_async_copy(src, dst, load.at[i]))
        loads[-1].start()
    rows[c, b, a] = jnp.zeros(rows.shape[3:], BF16)
    rows[c, b, a, 0:rows_local, 0:d] = branch_ref[...]
    rows[c, b, a, 0:rows_local, d : d + TABLE] = table_ref[...]
    pl.semaphore_wait(barrier, groups + 1)
    gather(rows, a, b, c, groups, send_z, send_y, send_d, recv)
    for copy in loads:
        copy.wait()

    everything = rows[:, :, :, :, 0:d].reshape(n * ROWS, d)
    table = rows[:, :, :, :, d : d + TABLE].reshape(n * ROWS, TABLE).astype(F32)
    total = jnp.sum(table, axis=-1, keepdims=True)
    total = jnp.where(total > 0.0, total, 1.0)
    lanes = lax.broadcasted_iota(jnp.int32, table.shape, 1)
    logit = jnp.sum(everything.astype(F32) * gate_w_ref[...].astype(F32), axis=-1, keepdims=True)
    branch_gate = jax.nn.sigmoid(logit)

    def ffn(gate, up, hid, wide):
        step = min(256, wide)
        for j in range(wide // step):
            cols = slice(j * step, (j + 1) * step)
            g = jnp.dot(everything, gate[:, cols], preferred_element_type=F32)
            u = jnp.dot(everything, up[:, cols], preferred_element_type=F32)
            hid[:, cols] = (jax.nn.silu(g) * u).astype(BF16)

    ffn(dg, du, hid_d, dg.shape[1])
    shares = []
    for e in range(experts_local):
        ffn(eg.at[e], eu.at[e], hid_e.at[e], eg.shape[2])
        mine = jnp.sum(jnp.where(lanes == me * experts_local + e, table, 0.0), axis=-1, keepdims=True)
        shares.append(mine / total)

    wide = d // CHUNKS
    copies = []
    for h in range(CHUNKS):
        cols = slice(h * wide, (h + 1) * wide)
        value = (jnp.dot(hid_d[...], dd[:, cols], preferred_element_type=F32) * branch_gate).astype(BF16).astype(F32)
        for e in range(experts_local):
            y = jnp.dot(hid_e[e], ed[e, :, cols], preferred_element_type=F32).astype(BF16).astype(F32)
            value = value + (shares[e] * y).astype(BF16).astype(F32)
        term[h] = value.astype(BF16).reshape(2, 2, groups, ROWS, wide)
        copies.append(push(term.at[h, 1 - c], recv1.at[h], s1.at[h], r1.at[h], d_peer))
    for h in range(CHUNKS):
        copies[h].wait_recv()
        part1[h] = (term[h, c].astype(F32) + recv1[h].astype(F32)).astype(BF16)
        copies.append(push(part1.at[h, 1 - b], recv2.at[h], s2.at[h], r2.at[h], y_peer))
    for h in range(CHUNKS):
        copies[CHUNKS + h].wait_recv()
        part2[h] = (part1[h, b].astype(F32) + recv2[h].astype(F32)).astype(BF16)
        for k in order:
            to = lax.rem(a + k, groups)
            copies.append(
                push(part2.at[h, to], recv3.at[h, a], s3.at[h, k], r3.at[h, a], device(to, b, c))
            )
    sums, square = [], 0.0
    for h in range(CHUNKS):
        value = part2[h, a].astype(F32)
        for k in order:
            src = lax.rem(a + k, groups)
            arrived(recv3.at[h, src], s3.at[h, k], r3.at[h, src], device(src, b, c))
            value = value + recv3[h, src].astype(F32)
        sums.append(value)
        square = square + jnp.sum(value * value, axis=-1, keepdims=True)
    scale = lax.rsqrt(square / d + 1e-06)
    for h in range(CHUNKS):
        cols = slice(h * wide, (h + 1) * wide)
        extra = (sums[h] * scale * gain_ref[:, cols])[0:rows_local]
        out_ref[:, cols] = (middle_ref[:, cols] + extra).astype(BF16)
    for copy in copies:
        copy.wait_send()


def branches(branch_in, table, middle, gain, gate_w, experts, dense, n):
    rows_local, d = branch_in.shape
    groups = n // 4
    vmem = pl.BlockSpec(memory_space=pltpu.VMEM)
    hbm = pl.BlockSpec(memory_space=pl.ANY)
    wide = d // CHUNKS
    dma = pltpu.SemaphoreType.DMA
    return pl.pallas_call(
        functools.partial(branch_kernel, n),
        out_shape=jax.ShapeDtypeStruct((rows_local, d), BF16),
        in_specs=[vmem] * 5 + [hbm] * 6,
        out_specs=vmem,
        scratch_shapes=[
            pltpu.VMEM((2, 2, groups, ROWS, d + TABLE), BF16),
            *[pltpu.VMEM(w.shape, BF16) for w in experts],
            *[pltpu.VMEM(w.shape, BF16) for w in dense],
            pltpu.VMEM((experts[0].shape[0], n * ROWS, experts[0].shape[2]), BF16),
            pltpu.VMEM((n * ROWS, dense[0].shape[1]), BF16),
            pltpu.VMEM((CHUNKS, 2, 2, groups, ROWS, wide), BF16),
            pltpu.VMEM((CHUNKS, 2, groups, ROWS, wide), BF16),
            pltpu.VMEM((CHUNKS, 2, groups, ROWS, wide), BF16),
            pltpu.VMEM((CHUNKS, groups, ROWS, wide), BF16),
            pltpu.VMEM((CHUNKS, groups, ROWS, wide), BF16),
            pltpu.VMEM((CHUNKS, groups, ROWS, wide), BF16),
            dma((6,)),
            dma((groups,)),
            dma((groups,)),
            dma((2, groups)),
            dma((2, 2, groups)),
            dma((CHUNKS,)),
            dma((CHUNKS,)),
            dma((CHUNKS,)),
            dma((CHUNKS,)),
            dma((CHUNKS, groups)),
            dma((CHUNKS, groups)),
        ],
        compiler_params=pltpu.CompilerParams(
            collective_id=1, has_side_effects=True, vmem_limit_bytes=48 * 2**20
        ),
        name="branches",
    )(branch_in, table, middle, gain, gate_w, *experts, *dense)


def local(
    resid, norm_gains, w_query, w_key, w_value, w_outgate, w_igate, w_fgate,
    igate_bias, fgate_bias, state_matrix, state_norm, state_max, w_mix_out,
    routes, route_scores, expert_gate, expert_up, expert_down,
    dense_gate, dense_up, dense_down, branch_weight,
):
    seqs_local = resid.shape[0]
    heads = state_matrix.shape[1]
    head_size = state_matrix.shape[2]
    devices_ep = lax.axis_size("ep")
    resid32 = resid.astype(F32)
    own_proj = project(
        resid, norm_gains[0:1], (w_query, w_key, w_value, w_outgate), devices_ep
    )[:, :seqs_local]
    normed = rms_scale(resid32, norm_gains[0]).astype(BF16)
    head_shape = (seqs_local, heads, head_size)
    query = own_proj[0].astype(F32).reshape(head_shape)
    key_heads = own_proj[1].astype(F32).reshape(head_shape) * head_size ** (-0.5)
    value_heads = own_proj[2].astype(F32).reshape(head_shape)
    outgate = own_proj[3].astype(F32).reshape(head_shape)
    ipre = jnp.dot(normed, w_igate, preferred_element_type=F32) + igate_bias
    fpre = jnp.dot(normed, w_fgate, preferred_element_type=F32) + fgate_bias
    logf = jax.nn.log_sigmoid(fpre)
    new_max = jnp.maximum(ipre, logf + state_max)
    keep_gain = jnp.exp(logf + state_max - new_max)
    write_gain = jnp.exp(ipre - new_max)
    new_matrix = (
        keep_gain[:, :, None, None] * state_matrix
        + write_gain[:, :, None, None] * value_heads[:, :, :, None] * key_heads[:, :, None, :]
    )
    new_norm = keep_gain[:, :, None] * state_norm + write_gain[:, :, None] * key_heads
    numer = jnp.einsum("shed,shd->she", new_matrix, query, precision=lax.Precision.HIGHEST)
    denom = jnp.sum(new_norm * query, axis=-1)
    cell = numer / jnp.maximum(jnp.abs(denom), 1.0)[:, :, None]
    gated = (
        (jax.nn.sigmoid(outgate) * cell).reshape(seqs_local, heads * head_size).astype(BF16)
    )
    mixed = jnp.dot(gated, w_mix_out, preferred_element_type=F32)
    middle = resid32 + rms_scale(mixed, norm_gains[1])
    branch_in = rms_scale(middle, norm_gains[2]).astype(BF16)
    lanes = jnp.arange(TABLE, dtype=jnp.int32)
    table = jnp.sum(
        jnp.where(routes[:, :, None] == lanes, route_scores.astype(F32)[:, :, None], 0.0), axis=1
    ).astype(BF16)
    out_stream = branches(
        branch_in, table, middle, norm_gains[3:4], branch_weight[None],
        (expert_gate, expert_up, expert_down), (dense_gate, dense_up, dense_down), devices_ep,
    )
    return (out_stream, new_matrix, new_norm, new_max)


def solution(mesh):
    rows = ("grp", "ep")
    placed = (
        P(rows, None),
        P(),
        P(None, "ep"),
        P(None, "ep"),
        P(None, "ep"),
        P(None, "ep"),
        P(),
        P(),
        P(),
        P(),
        P(rows, None, None, None),
        P(rows, None, None),
        P(rows, None),
        P(),
        P(rows, None),
        P(rows, None),
        P("ep", None, None),
        P("ep", None, None),
        P("ep", None, None),
        P(None, "ep"),
        P(None, "ep"),
        P("ep", None),
        P(),
    )
    return jax.shard_map(
        local,
        mesh=mesh,
        in_specs=placed,
        out_specs=(
            P(rows, None),
            P(rows, None, None, None),
            P(rows, None, None),
            P(rows, None),
        ),
        check_vma=False,
    )
```

time: 162 us -> 83.7 us (0.52)
  blocking collectives: 89.8 us -> 0 us
  Pallas kernels: 0 us -> 55.5 us
  starting transfers between devices: 15.9 us -> 0 us
  matrix products: 21.1 us -> 9.14 us
  waiting for transfers between devices: 10.6 us -> 0 us
  other arithmetic: 10.4 us -> 8.1 us
    pallas_call x0 -> x2, Pallas kernels: none -> 55.5 us  [the longest x1 31.2 us: branches(): pl.pallas_call(functools.partial(branch_kernel, n), out_shape=jax.ShapeDt...]
    all_gather x2 -> x0, blocking collectives: 49.7 us -> none  [the longest x1 27.6 us: local(): row_piece = lax.all_gather(normed, 'ep', axis=0, tiled=True)]
    unnamed x1 -> x0, blocking collectives: 40.1 us -> none
    dot_general x14 -> x3, matrix products: 16.1 us -> 1.98 us  [the longest x1 1 us: local(): fpre = jnp.dot(normed, w_fgate, preferred_element_type=F32) + fgate_bias]
    all_to_all x3 -> x0, starting transfers between devices: 10.7 us -> none  [the longest x1 3.69 us: exchanged_experts(): lax.all_to_all(outgoing, 'ep', split_axis=0, concat_axis=1, tiled=True)]
    all_to_all x3 -> x0, waiting for transfers between devices: 10 us -> none  [the longest x1 5.94 us: local(): lax.all_to_all(projected, 'ep', split_axis=0, concat_axis=2, tiled=True)]
    unnamed x4 -> x0, starting transfers between devices: 5.17 us -> none
    unnamed x3 -> x0, other arithmetic: 2.45 us -> none
  transfers between devices with their start and end apart: 7 -> 0, of which waited for: 3 -> 0; matrix products, arithmetic and copies ran while one was open for 29% -> 0% of each run, Pallas kernels for 0% -> 0%
where the time goes in v1:
time: 83.7 us; the launch traced here: 83.2 us
  Pallas kernels  55.5 us (66%)
  local copies, waits for them, and re-layouts  9.5 us (11%)
  matrix products  9.14 us (11%)
  other arithmetic  8.1 us (10%)
  between operations  0.93 us (1%)
    pallas_call x1, Pallas kernels, branches(): pl.pallas_call(functools.partial(branch_kernel, n), out_shape=jax.ShapeDt...  31.2 us
    pallas_call x1, Pallas kernels, project(): pl.pallas_call(functools.partial(project_kernel, n), out_shape=jax.ShapeD...  24.3 us
    unnamed x36, local copies, waits for them, and re-layouts  8.17 us
    dot_general x1, matrix products, local(): jnp.einsum('shed,shd->she', new_matrix, query, precision=lax.Precision.HI...  7.16 us
    add x1, other arithmetic, local(): keep_gain[:, :, None, None] * state_matrix  6.65 us

profile of v1, /device:TPU:0, one launch (start us, length us, event | category | flops | bytes accessed | tf_op | source)
XLA Modules:
  0.0 83.2 jit_solution(603702559328089357)
XLA Ops:
  0.6 0.0 copy-start
  0.6 0.0 copy-start.11
  0.7 0.0 copy-start.6
  0.7 0.9 %fusion.13 = (f32[1,2048]{1,0:T(1,128)S(1)}, f32[1,2048]{1,0:T(1,128)S(1)}, f32[1,2048]{1,0:T(1,128)S(1)}, f32[1,2048]{1,0:T(1,128)S(1)}) fusion(f32[4,2048]{1,0:T(4,128)} %param.24), kind=kLoop, calls=%fused_computation.35 | loop fusion | bytes 65536 | tf_op jit(solution)/shard_map/slice | solution.py:338
  1.6 1.2 %copy.47.wq_ref = bf16[2048,64]{1,0:T(8,128)(2,1)S(1)} copy(bf16[2048,64]{0,1:T(8,128)(2,1)} %param.25) | data formatting | bytes 524288 | tf_op args[2]
  2.8 1.2 %copy.48.wk_ref = bf16[2048,64]{1,0:T(8,128)(2,1)S(1)} copy(bf16[2048,64]{0,1:T(8,128)(2,1)} %param.26) | data formatting | bytes 524288 | tf_op args[3]
  4.1 1.2 %copy.49.wv_ref = bf16[2048,64]{1,0:T(8,128)(2,1)S(1)} copy(bf16[2048,64]{0,1:T(8,128)(2,1)} %param.27) | data formatting | bytes 524288 | tf_op args[4]
  5.3 1.2 %copy.50.wo_ref = bf16[2048,64]{1,0:T(8,128)(2,1)S(1)} copy(bf16[2048,64]{0,1:T(8,128)(2,1)} %param.28) | data formatting | bytes 524288 | tf_op args[5]
  6.5 0.0 copy-start.3
  6.6 0.8 %copy-done.3 = bf16[12,2048]{1,0:T(8,128)(2,1)S(1)} copy-done((bf16[12,2048]{1,0:T(8,128)(2,1)S(1)}, bf16[12,2048]{1,0:T(8,128)(2,1)}, u32[]{:S(2)}) %copy-start.3) | copy-done | bytes 49176
  7.4 24.3 %project.1 = bf16[4,16,1024]{2,1,0:T(8,128)(2,1)S(1)} custom-call(bf16[12,2048]{1,0:T(8,128)(2,1)S(1)} %copy-done.3, f32[1,2048]{1,0:T(1,128)S(1)} %get-tuple-element.17.gain_ref, bf16[2048,64]{1,0:T(8,128)(2,1)S(1)} %copy.47.wq_ref, bf16[2048,64]{1,0:T(8,128)(2,1)S(1)} %copy.48.wk_ref, bf16[2048,64]{1,0:T(8,128)(2,1)S(1)} %copy.49.wv_ref, ...), custom_call_target="tpu_custom_call" | custom-call | tf_op jit(solution)/shard_map/project/pallas_call | solution.py:133
  31.8 0.1 fusion.1
  32.0 1.0 %fusion.9 = f32[12,8]{0,1:T(8,128)S(1)} fusion(f32[12,8]{0,1:T(8,128)} %param.35, bf16[2048,8]{0,1:T(8,128)(2,1)} %param.30, bf16[12,2048]{1,0:T(8,128)(2,1)S(1)} %copy-done.3, f32[2048]{0:T(1024)S(1)} %bitcast.30, f32[12]{0:T(128)S(1)} %add_rsqrt_fusion.2, f32[8]{0:T(128)} %param.32), kind=kOutput, calls=%fused_computation.27 | convolution fusion | flops 492480 | bytes 90960 | tf_op jit(solution)/shard_map/dot_general | solution.py:314
  33.0 0.0 copy-done
  33.0 0.0 copy-done.11
  33.0 0.2 broadcast_multiply_fusion
  33.2 0.0 copy-start.8
  33.2 0.1 copy.54
  33.3 0.1 copy.51
  33.4 0.1 copy.52
  33.5 0.0 copy-done.6
  33.5 0.7 multiply_reduce_fusion.2
  34.2 6.7 %multiply_add_fusion = f32[12,8,128,128]{3,2,1,0:T(8,128)} fusion(f32[12,8,128,128]{3,2,1,0:T(8,128)} %param.33, f32[12,8,128]{2,1,0:T(8,128)S(1)} %get-tuple-element.14, f32[12,8,128]{2,1,0:T(8,128)S(1)} %get-tuple-element.21, f32[12,8]{1,0:T(8,128)S(1)} %copy.51), kind=kLoop, calls=%fused_computation | loop fusion | flops 4718592 | bytes 12681600 | tf_op jit(solution)/shard_map/add | solution.py:320
  40.9 0.0 copy-done.8
  40.9 0.0 copy-start.4
  40.9 0.0 copy-start.10
  40.9 0.0 copy-start.9
  40.9 0.0 copy-start.7
  40.9 0.0 copy-start.1
  41.0 0.0 copy-start.5
  41.0 7.2 %fusion.14 = f32[12,8,1,128]{3,2,1,0:T(1,128)S(1)} fusion(f32[12,8,128,128]{3,2,1,0:T(8,128)} %multiply_add_fusion, bf16[12,8,128,1]{2,3,1,0:T(2,128)(2,1)S(1)} %reshape.89), kind=kOutput, calls=%fused_computation.36 | convolution fusion | flops 18874368 | bytes 6365184 | tf_op jit(solution)/shard_map/shed,shd->she/dot_general | solution.py:324
  48.1 0.1 fusion.4
  48.3 0.0 copy-done.5
  48.3 0.8 multiply_reduce_fusion.1
  49.1 0.0 copy-done.4
  49.1 0.2 multiply_reduce_fusion
  49.3 0.1 multiply_convert_fusion.branch_ref
  49.4 0.0 copy-done.10
  49.4 0.1 copy.56
  49.5 0.0 copy-done.9
  49.5 0.1 copy.55
  49.6 0.1 fusion.7.table_ref
  49.7 0.0 copy-done.7
  49.8 0.0 copy-done.1
  49.8 0.0 copy-start.2
  49.8 1.6 %copy-done.2 = bf16[1,2048,512]{2,1,0:T(8,128)(2,1)S(1)} copy-done((bf16[1,2048,512]{2,1,0:T(8,128)(2,1)S(1)}, bf16[1,2048,512]{2,1,0:T(8,128)(2,1)}, u32[]{:S(2)}) %copy-start.2) | copy-done | bytes 2097176
  51.4 31.2 %branches.1 = bf16[12,2048]{1,0:T(8,128)(2,1)S(1)} custom-call(bf16[12,2048]{1,0:T(8,128)(2,1)S(1)} %multiply_convert_fusion.branch_ref, bf16[12,128]{1,0:T(8,128)(2,1)S(1)} %fusion.7.table_ref, f32[12,2048]{1,0:T(8,128)S(1)} %get-tuple-element.5.middle_ref, f32[1,2048]{1,0:T(1,128)S(1)} %get-tuple-element.15.gain_ref, ...), custom_call_target="tpu_custom_call" | custom-call | tf_op jit(solution)/shard_map/branches/pallas_call | solution.py:257
  82.6 0.6 copy.65
  (15 shorter events, 0.2 us)
Async XLA Ops:
  0.6 32.3 %copy-start = (bf16[2048,8]{0,1:T(8,128)(2,1)S(1)}, bf16[2048,8]{0,1:T(8,128)(2,1)}, u32[]{:S(2)}) copy-start(bf16[2048,8]{0,1:T(8,128)(2,1)} %param.29) | copy-start | bytes 98308
  0.6 32.3 %copy-start.11 = (f32[8]{0:T(128)S(1)}, f32[8]{0:T(128)}, u32[]{:S(2)}) copy-start(f32[8]{0:T(128)} %param.31) | copy-start | bytes 100
  0.7 32.9 %copy-start.6 = (f32[12,8,128]{2,1,0:T(8,128)S(1)}, f32[12,8,128]{2,1,0:T(8,128)}, u32[]{:S(2)}) copy-start(f32[12,8,128]{2,1,0:T(8,128)} %param.34) | copy-start | bytes 147460
  6.5 0.8 %copy-start.3 = (bf16[12,2048]{1,0:T(8,128)(2,1)S(1)}, bf16[12,2048]{1,0:T(8,128)(2,1)}, u32[]{:S(2)}) copy-start(bf16[12,2048]{1,0:T(8,128)(2,1)} %resid_ref.1) | copy-start | bytes 147460
  33.2 7.7 %copy-start.8 = (f32[12,8]{0,1:T(8,128)}, f32[12,8]{0,1:T(8,128)S(1)}, u32[]{:S(2)}) copy-start(f32[12,8]{0,1:T(8,128)S(1)} %get-tuple-element.29) | copy-start | bytes 1156
  40.9 8.2 %copy-start.4 = (bf16[12,2048]{1,0:T(8,128)(2,1)S(1)}, bf16[12,2048]{1,0:T(8,128)(2,1)}, u32[]{:S(2)}) copy-start(bf16[12,2048]{1,0:T(8,128)(2,1)} %resid_ref.1) | copy-start | bytes 147460
  40.9 8.5 %copy-start.10 = (bf16[12,2]{0,1:T(2,128)(2,1)S(1)}, bf16[12,2]{0,1:T(2,128)(2,1)}, u32[]{:S(2)}) copy-start(bf16[12,2]{0,1:T(2,128)(2,1)} %param.38) | copy-start | bytes 148
  40.9 8.6 %copy-start.9 = (s32[12,2]{0,1:T(2,128)S(1)}, s32[12,2]{0,1:T(2,128)}, u32[]{:S(2)}) copy-start(s32[12,2]{0,1:T(2,128)} %param.37) | copy-start | bytes 292
  40.9 8.8 %copy-start.7 = (bf16[2048]{0:T(1024)(128)(2,1)S(1)}, bf16[2048]{0:T(1024)(128)(2,1)}, u32[]{:S(2)}) copy-start(bf16[2048]{0:T(1024)(128)(2,1)} %param.45) | copy-start | bytes 12292
  40.9 8.8 %copy-start.1 = (bf16[1,2048,512]{2,1,0:T(8,128)(2,1)S(1)}, bf16[1,2048,512]{2,1,0:T(8,128)(2,1)}, u32[]{:S(2)}) copy-start(bf16[1,2048,512]{2,1,0:T(8,128)(2,1)} %eg_hbm.1) | copy-start | bytes 6291460
  41.0 7.3 %copy-start.5 = (bf16[1024,2048]{1,0:T(8,128)(2,1)S(1)}, bf16[1024,2048]{1,0:T(8,128)(2,1)}, u32[]{:S(2)}) copy-start(bf16[1024,2048]{1,0:T(8,128)(2,1)} %param.36) | copy-start | bytes 12582916
  49.8 1.6 %copy-start.2 = (bf16[1,2048,512]{2,1,0:T(8,128)(2,1)S(1)}, bf16[1,2048,512]{2,1,0:T(8,128)(2,1)}, u32[]{:S(2)}) copy-start(bf16[1,2048,512]{2,1,0:T(8,128)(2,1)} %eu_hbm.1) | copy-start | bytes 6291460

commit v2 on v1

--- a/solution.py
+++ b/solution.py
@@ -12,11 +12,20 @@
 BF16 = jnp.bfloat16
 ROWS = 16
 TABLE = 128
+VMEM_BYTES = 61 * 2**20
 CHUNKS = 4
 
 
 def rms_scale(values, gains):
     return values * lax.rsqrt(jnp.mean(values * values, axis=-1, keepdims=True) + 1e-06) * gains
+
+
+def spent(us):
+    return pl.CostEstimate(flops=us * 10**9, bytes_accessed=us * 2 * 10**6, transcendentals=0)
+
+
+def dot_t(left, right):
+    return lax.dot_general(left, right, (((1,), (1,)), ((), ())), preferred_element_type=F32)
 
 
 def place():
@@ -82,26 +91,34 @@
 
 def project_kernel(
     n, resid_ref, gain_ref, wq_ref, wk_ref, wv_ref, wo_ref, out_ref,
-    rows, local, landed, send_z, send_y, send_d, recv, send_x, recv_x,
+    wq, wk, wv, wo, rows, local, landed, load, send_z, send_y, send_d, recv, send_x, recv_x,
 ):
     groups = n // 4
     a, b, c = place()
     me = lax.axis_index("ep")
     rows_local = resid_ref.shape[0]
-    width = wq_ref.shape[1]
+    width = wq.shape[0]
     barrier = pltpu.get_barrier_semaphore()
     for k in range(1, n):
         pl.semaphore_signal(
             barrier, inc=1, device_id={"ep": lax.rem(me + k, n)}, device_id_type=MESH
         )
+    loads = [
+        pltpu.make_async_copy(src, dst, load.at[i])
+        for i, (src, dst) in enumerate(((wq_ref, wq), (wk_ref, wk), (wv_ref, wv), (wo_ref, wo)))
+    ]
+    for copy in loads:
+        copy.start()
     normed = rms_scale(resid_ref[...].astype(F32), gain_ref[...]).astype(BF16)
     rows[c, b, a] = jnp.zeros(rows.shape[3:], BF16)
     rows[c, b, a, 0:rows_local, :] = normed
     pl.semaphore_wait(barrier, n - 1)
     gather(rows, a, b, c, groups, send_z, send_y, send_d, recv)
     everything = rows[...].reshape(n * ROWS, rows.shape[-1])
-    for m, w_ref in enumerate((wq_ref, wk_ref, wv_ref, wo_ref)):
-        piece = jnp.dot(everything, w_ref[...], preferred_element_type=F32).astype(BF16)
+    for copy in loads:
+        copy.wait()
+    for m, w_ref in enumerate((wq, wk, wv, wo)):
+        piece = dot_t(everything, w_ref[...]).astype(BF16)
         local[:, :, :, :, m * width : (m + 1) * width] = piece.reshape(2, 2, groups, ROWS, width)
     sent = []
     for k in range(1, n):
@@ -127,18 +144,20 @@
 
 def project(resid, gain, weights, n):
     rows_local, d = resid.shape
-    width = weights[0].shape[1]
+    width = weights[0].shape[0]
     groups = n // 4
     vmem = pl.BlockSpec(memory_space=pltpu.VMEM)
     return pl.pallas_call(
         functools.partial(project_kernel, n),
         out_shape=jax.ShapeDtypeStruct((4, ROWS, n * width), BF16),
-        in_specs=[vmem] * 6,
+        in_specs=[vmem] * 2 + [pl.BlockSpec(memory_space=pltpu.HBM)] * 4,
         out_specs=vmem,
         scratch_shapes=[
+            *[pltpu.VMEM(w.shape, BF16) for w in weights],
             pltpu.VMEM((2, 2, groups, ROWS, d), BF16),
             pltpu.VMEM((2, 2, groups, ROWS, 4 * width), BF16),
             pltpu.VMEM((2, 2, groups, ROWS, 4 * width), BF16),
+            pltpu.SemaphoreType.DMA((4,)),
             pltpu.SemaphoreType.DMA((groups,)),
             pltpu.SemaphoreType.DMA((groups,)),
             pltpu.SemaphoreType.DMA((2, groups)),
@@ -147,23 +166,114 @@
             pltpu.SemaphoreType.DMA((2, 2, groups)),
         ],
         compiler_params=pltpu.CompilerParams(
-            collective_id=0, has_side_effects=True, vmem_limit_bytes=32 * 2**20
+            collective_id=0, has_side_effects=True, vmem_limit_bytes=VMEM_BYTES
         ),
+        cost_estimate=spent(20),
         name="project",
     )(resid, gain, *weights)
 
 
+def cell_kernel(
+    proj_ref, resid_ref, gain_ref, wi_ref, wf_ref, bi_ref, bf_ref, max_ref, norm_ref, state_hbm,
+    matrix_hbm, norm_out, max_out, gated_ref,
+    old, fresh, q3, k3, wv3, keep3, numer3, load, sem,
+):
+    count, heads, size, _ = old.shape
+
+    def loading(s):
+        return pltpu.make_async_copy(state_hbm.at[s], old.at[s], load.at[s])
+
+    for s in range(count):
+        loading(s).start()
+    normed = rms_scale(resid_ref[...].astype(F32), gain_ref[...]).astype(BF16)
+    ipre = dot_t(normed, wi_ref[...]) + bi_ref[...]
+    fpre = dot_t(normed, wf_ref[...]) + bf_ref[...]
+    logf = jnp.minimum(fpre, 0.0) - jnp.log1p(jnp.exp(-jnp.abs(fpre)))
+    old_max = logf + max_ref[...]
+    new_max = jnp.maximum(ipre, old_max)
+    max_out[...] = new_max
+    keep = jnp.exp(old_max - new_max)
+    write = jnp.exp(ipre - new_max)
+    denoms = []
+    for h in range(heads):
+        cols = slice(h * size, (h + 1) * size)
+        q = proj_ref[0, 0:count, cols].astype(F32)
+        k = proj_ref[1, 0:count, cols].astype(F32) * size ** (-0.5)
+        v = proj_ref[2, 0:count, cols].astype(F32)
+        keep_h, write_h = keep[:, h : h + 1], write[:, h : h + 1]
+        new_norm = keep_h * norm_ref[:, h, :] + write_h * k
+        norm_out[:, h, :] = new_norm
+        denoms.append(jnp.maximum(jnp.abs(jnp.sum(new_norm * q, axis=-1, keepdims=True)), 1.0))
+        q3[:, h, :] = q
+        k3[:, h, :] = k
+        wv3[:, h, :] = write_h * v
+        keep3[:, h, :] = jnp.broadcast_to(keep_h, (count, size))
+
+    def sequence(s, carry):
+        q, k, kept = q3[s], k3[s], keep3[s]
+        loading(s).wait()
+        column = wv3[s].T
+        lane = lax.broadcasted_iota(jnp.int32, (size, heads), 1)
+        numer = jnp.zeros((size, heads), F32)
+        for h in range(heads):
+            new = (
+                old[s, h] * kept[h : h + 1, :] + column[:, h : h + 1] * k[h : h + 1, :]
+            )
+            fresh[s, h] = new
+            read = jnp.sum(new * q[h : h + 1, :], axis=-1, keepdims=True)
+            numer = jnp.where(lane == h, read, numer)
+        pltpu.make_async_copy(fresh.at[s], matrix_hbm.at[s], sem.at[s]).start()
+        numer3[s] = numer.T
+        return carry
+
+    lax.fori_loop(0, count, sequence, 0)
+    for h in range(heads):
+        cols = slice(h * size, (h + 1) * size)
+        outgate = proj_ref[3, 0:count, cols].astype(F32)
+        cell = numer3[:, h, :] / denoms[h]
+        gated_ref[:, cols] = (jax.nn.sigmoid(outgate) * cell).astype(BF16)
+    for s in range(count):
+        pltpu.make_async_copy(fresh.at[s], matrix_hbm.at[s], sem.at[s]).wait()
+
+
+def cell_update(proj, resid, gain, gates, biases, state_max, state_norm, state):
+    count, heads, size, _ = state.shape
+    vmem = pl.BlockSpec(memory_space=pltpu.VMEM)
+    small = pltpu.VMEM((count, heads, size), F32)
+    return pl.pallas_call(
+        cell_kernel,
+        out_shape=(
+            jax.ShapeDtypeStruct(state.shape, F32),
+            jax.ShapeDtypeStruct(state_norm.shape, F32),
+            jax.ShapeDtypeStruct(state_max.shape, F32),
+            jax.ShapeDtypeStruct((count, heads * size), BF16),
+        ),
+        in_specs=[vmem] * 9 + [pl.BlockSpec(memory_space=pl.ANY)],
+        out_specs=(pl.BlockSpec(memory_space=pl.ANY), vmem, vmem, vmem),
+        scratch_shapes=[
+            pltpu.VMEM(state.shape, F32),
+            pltpu.VMEM(state.shape, F32),
+            small, small, small, small, small,
+            pltpu.SemaphoreType.DMA((count,)),
+            pltpu.SemaphoreType.DMA((count,)),
+        ],
+        compiler_params=pltpu.CompilerParams(vmem_limit_bytes=VMEM_BYTES),
+        cost_estimate=spent(6),
+        name="cell_update",
+    )(proj, resid, gain, *gates, *biases, state_max, state_norm, state)
+
+
 def branch_kernel(
-    n, branch_ref, table_ref, middle_ref, gain_ref, gate_w_ref,
+    n, gated_ref, resid_ref, table_ref, gains_ref, gate_w_ref, mix_hbm,
     eg_hbm, eu_hbm, ed_hbm, dg_hbm, du_hbm, dd_hbm, out_ref,
-    rows, eg, eu, ed, dg, du, dd, hid_e, hid_d,
+    middle, mix, rows, eg, eu, ed, dg, du, dd, hid_e, hid_d,
     term, recv1, part1, recv2, part2, recv3,
     load, send_z, send_y, send_d, recv, s1, r1, s2, r2, s3, r3,
 ):
     groups = n // 4
     a, b, c = place()
     me = lax.axis_index("ep")
-    rows_local, d = branch_ref.shape
+    rows_local, d = resid_ref.shape
     experts_local = eg.shape[0]
     order = near_first(groups)
     y_peer, d_peer = device(a, 1 - b, c), device(a, b, 1 - c)
@@ -172,20 +282,25 @@
         pl.semaphore_signal(barrier, inc=1, device_id=to, device_id_type=MESH)
     loads = []
     for i, (src, dst) in enumerate(
-        ((dg_hbm, dg), (du_hbm, du), (eg_hbm, eg), (eu_hbm, eu), (dd_hbm, dd), (ed_hbm, ed))
+        ((mix_hbm, mix), (dg_hbm, dg), (du_hbm, du), (eg_hbm, eg), (eu_hbm, eu), (dd_hbm, dd), (ed_hbm, ed))
     ):
         loads.append(pltpu.make_async_copy(src, dst, load.at[i]))
         loads[-1].start()
     rows[c, b, a] = jnp.zeros(rows.shape[3:], BF16)
-    rows[c, b, a, 0:rows_local, 0:d] = branch_ref[...]
-    rows[c, b, a, 0:rows_local, d : d + TABLE] = table_ref[...]
+    loads[0].wait()
+    mixed = jnp.dot(gated_ref[...], mix[...], preferred_element_type=F32)
+    stream = resid_ref[...].astype(F32) + rms_scale(mixed, gains_ref[1:2, :])
+    middle[...] = stream
+    lanes_all = table_ref.shape[1]
+    rows[c, b, a, 0:rows_local, 0:d] = rms_scale(stream, gains_ref[2:3, :]).astype(BF16)
+    rows[c, b, a, 0:rows_local, d : d + lanes_all] = table_ref[...]
     pl.semaphore_wait(barrier, groups + 1)
     gather(rows, a, b, c, groups, send_z, send_y, send_d, recv)
-    for copy in loads:
+    for copy in loads[1:]:
         copy.wait()
 
     everything = rows[:, :, :, :, 0:d].reshape(n * ROWS, d)
-    table = rows[:, :, :, :, d : d + TABLE].reshape(n * ROWS, TABLE).astype(F32)
+    table = rows[:, :, :, :, d : d + lanes_all].reshape(n * ROWS, lanes_all).astype(F32)
     total = jnp.sum(table, axis=-1, keepdims=True)
     total = jnp.where(total > 0.0, total, 1.0)
     lanes = lax.broadcasted_iota(jnp.int32, table.shape, 1)
@@ -241,26 +356,28 @@
     scale = lax.rsqrt(square / d + 1e-06)
     for h in range(CHUNKS):
         cols = slice(h * wide, (h + 1) * wide)
-        extra = (sums[h] * scale * gain_ref[:, cols])[0:rows_local]
-        out_ref[:, cols] = (middle_ref[:, cols] + extra).astype(BF16)
+        extra = (sums[h] * scale * gains_ref[3:4, cols])[0:rows_local]
+        out_ref[:, cols] = (middle[:, cols] + extra).astype(BF16)
     for copy in copies:
         copy.wait_send()
 
 
-def branches(branch_in, table, middle, gain, gate_w, experts, dense, n):
-    rows_local, d = branch_in.shape
+def branches(gated, resid, table, gains, gate_w, w_mix, experts, dense, n):
+    rows_local, d = resid.shape
     groups = n // 4
     vmem = pl.BlockSpec(memory_space=pltpu.VMEM)
-    hbm = pl.BlockSpec(memory_space=pl.ANY)
+    hbm = pl.BlockSpec(memory_space=pltpu.HBM)
     wide = d // CHUNKS
     dma = pltpu.SemaphoreType.DMA
     return pl.pallas_call(
         functools.partial(branch_kernel, n),
         out_shape=jax.ShapeDtypeStruct((rows_local, d), BF16),
-        in_specs=[vmem] * 5 + [hbm] * 6,
+        in_specs=[vmem] * 5 + [hbm] * 7,
         out_specs=vmem,
         scratch_shapes=[
-            pltpu.VMEM((2, 2, groups, ROWS, d + TABLE), BF16),
+            pltpu.VMEM((rows_local, d), F32),
+            pltpu.VMEM(w_mix.shape, BF16),
+            pltpu.VMEM((2, 2, groups, ROWS, d + table.shape[1]), BF16),
             *[pltpu.VMEM(w.shape, BF16) for w in experts],
             *[pltpu.VMEM(w.shape, BF16) for w in dense],
             pltpu.VMEM((experts[0].shape[0], n * ROWS, experts[0].shape[2]), BF16),
@@ -271,7 +388,7 @@
             pltpu.VMEM((CHUNKS, groups, ROWS, wide), BF16),
             pltpu.VMEM((CHUNKS, groups, ROWS, wide), BF16),
             pltpu.VMEM((CHUNKS, groups, ROWS, wide), BF16),
-            dma((6,)),
+            dma((7,)),
             dma((groups,)),
             dma((groups,)),
             dma((2, groups)),
@@ -284,10 +401,11 @@
             dma((CHUNKS, groups)),
         ],
         compiler_params=pltpu.CompilerParams(
-            collective_id=1, has_side_effects=True, vmem_limit_bytes=48 * 2**20
+            collective_id=1, has_side_effects=True, vmem_limit_bytes=VMEM_BYTES
         ),
+        cost_estimate=spent(25),
         name="branches",
-    )(branch_in, table, middle, gain, gate_w, *experts, *dense)
+    )(gated, resid, table, gains, gate_w, w_mix, *experts, *dense)
 
 
 def local(
@@ -296,46 +414,21 @@
     routes, route_scores, expert_gate, expert_up, expert_down,
     dense_gate, dense_up, dense_down, branch_weight,
 ):
-    seqs_local = resid.shape[0]
-    heads = state_matrix.shape[1]
-    head_size = state_matrix.shape[2]
     devices_ep = lax.axis_size("ep")
-    resid32 = resid.astype(F32)
-    own_proj = project(
-        resid, norm_gains[0:1], (w_query, w_key, w_value, w_outgate), devices_ep
-    )[:, :seqs_local]
-    normed = rms_scale(resid32, norm_gains[0]).astype(BF16)
-    head_shape = (seqs_local, heads, head_size)
-    query = own_proj[0].astype(F32).reshape(head_shape)
-    key_heads = own_proj[1].astype(F32).reshape(head_shape) * head_size ** (-0.5)
-    value_heads = own_proj[2].astype(F32).reshape(head_shape)
-    outgate = own_proj[3].astype(F32).reshape(head_shape)
-    ipre = jnp.dot(normed, w_igate, preferred_element_type=F32) + igate_bias
-    fpre = jnp.dot(normed, w_fgate, preferred_element_type=F32) + fgate_bias
-    logf = jax.nn.log_sigmoid(fpre)
-    new_max = jnp.maximum(ipre, logf + state_max)
-    keep_gain = jnp.exp(logf + state_max - new_max)
-    write_gain = jnp.exp(ipre - new_max)
-    new_matrix = (
-        keep_gain[:, :, None, None] * state_matrix
-        + write_gain[:, :, None, None] * value_heads[:, :, :, None] * key_heads[:, :, None, :]
-    )
-    new_norm = keep_gain[:, :, None] * state_norm + write_gain[:, :, None] * key_heads
-    numer = jnp.einsum("shed,shd->she", new_matrix, query, precision=lax.Precision.HIGHEST)
-    denom = jnp.sum(new_norm * query, axis=-1)
-    cell = numer / jnp.maximum(jnp.abs(denom), 1.0)[:, :, None]
-    gated = (
-        (jax.nn.sigmoid(outgate) * cell).reshape(seqs_local, heads * head_size).astype(BF16)
-    )
-    mixed = jnp.dot(gated, w_mix_out, preferred_element_type=F32)
-    middle = resid32 + rms_scale(mixed, norm_gains[1])
-    branch_in = rms_scale(middle, norm_gains[2]).astype(BF16)
-    lanes = jnp.arange(TABLE, dtype=jnp.int32)
+    proj = project(
+        resid, norm_gains[0:1], (w_query.T, w_key.T, w_value.T, w_outgate.T), devices_ep
+    )
+    new_matrix, new_norm, new_max, gated = cell_update(
+        proj, resid, norm_gains[0:1], (w_igate.T, w_fgate.T),
+        (igate_bias[None], fgate_bias[None]), state_max, state_norm, state_matrix,
+    )
+    experts = expert_gate.shape[0] * devices_ep
+    lanes = jnp.arange(-(-experts // TABLE) * TABLE, dtype=jnp.int32)
     table = jnp.sum(
         jnp.where(routes[:, :, None] == lanes, route_scores.astype(F32)[:, :, None], 0.0), axis=1
     ).astype(BF16)
     out_stream = branches(
-        branch_in, table, middle, norm_gains[3:4], branch_weight[None],
+        gated, resid, table, norm_gains, branch_weight[None], w_mix_out,
         (expert_gate, expert_up, expert_down), (dense_gate, dense_up, dense_down), devices_ep,
     )
     return (out_stream, new_matrix, new_norm, new_max)

time: 83.7 us -> 81.6 us (0.975)
  Pallas kernels: 55.5 us -> 74.9 us
  matrix products: 9.14 us -> 0 us
  other arithmetic: 8.1 us -> 0.7 us
  local copies, waits for them, and re-layouts: 9.5 us -> 4.99 us
    pallas_call x0 -> x1, Pallas kernels: none -> 14.7 us  [cell_update(): pl.pallas_call(cell_kernel, out_shape=(jax.ShapeDtypeStruct(state.shape,...]
    dot_general x4 -> x0, matrix products: 9.14 us -> none  [the longest x1 7.16 us: local(): jnp.einsum('shed,shd->she', new_matrix, query, precision=lax.Precision.HI...]
    add x1 -> x0, other arithmetic: 6.65 us -> none  [local(): keep_gain[:, :, None, None] * state_matrix]
    unnamed x36 -> x14, local copies, waits for them, and re-layouts: 8.17 us -> 2.93 us
    pallas_call x1, Pallas kernels: 31.2 us -> 34.3 us  [branches(): pl.pallas_call(functools.partial(branch_kernel, n), out_shape=jax.ShapeDt...]
    pallas_call x1, Pallas kernels: 24.3 us -> 25.9 us  [project(): pl.pallas_call(functools.partial(project_kernel, n), out_shape=jax.ShapeD...]
    reduce_sum x3 -> x0, other arithmetic: 1.06 us -> none  [the longest x1 0.72 us: local(): denom = jnp.sum(new_norm * query, axis=-1)]
where the time goes in v2:
time: 81.6 us; the launch traced here: 81.2 us
  Pallas kernels  74.9 us (92%)
  local copies, waits for them, and re-layouts  4.99 us (6%)
    pallas_call x1, Pallas kernels, branches(): pl.pallas_call(functools.partial(branch_kernel, n), out_shape=jax.ShapeDt...  34.3 us
    pallas_call x1, Pallas kernels, project(): pl.pallas_call(functools.partial(project_kernel, n), out_shape=jax.ShapeD...  25.9 us
    pallas_call x1, Pallas kernels, cell_update(): pl.pallas_call(cell_kernel, out_shape=(jax.ShapeDtypeStruct(state.shape,...  14.7 us
    unnamed x14, local copies, waits for them, and re-layouts  2.93 us

profile of v2, /device:TPU:0, one launch (start us, length us, event | category | flops | bytes accessed | tf_op | source)
XLA Modules:
  0.0 81.2 jit_solution(16834915107586890623)
XLA Ops:
  0.6 1.4 %slice.4.gain_ref = f32[1,2048]{1,0:T(1,128)} slice(f32[4,2048]{1,0:T(4,128)} %gains_ref.1), slice={[0:1], [0:2048]} | slice | bytes 16384 | tf_op jit(solution)/shard_map/slice | solution.py:419
  2.0 0.0 copy-start.1
  2.0 25.9 %project.1.proj_ref = bf16[4,16,1024]{2,1,0:T(8,128)(2,1)} custom-call(bf16[12,2048]{1,0:T(8,128)(2,1)} %resid_ref.5, f32[1,2048]{1,0:T(1,128)} %slice.4.gain_ref, bf16[64,2048]{1,0:T(8,128)(2,1)} %bitcast.8, bf16[64,2048]{1,0:T(8,128)(2,1)} %bitcast.9, bf16[64,2048]{1,0:T(8,128)(2,1)} %bitcast.10, bf16[64,2048]{1,0:T(8,128)(2,1)} %bitcast.11), custom_call_target="tpu_custom_call" | custom-call | flops 20000000000 | bytes 40000000 | tf_op jit(solution)/shard_map/project/pallas_call | solution.py:150
  27.9 0.0 copy-done.1
  27.9 0.7 copy.31.max_ref
  28.6 0.0 copy-start.3
  28.6 0.0 copy-start.4
  28.6 0.0 copy-start.2
  28.6 14.7 %cell_update.1 = (f32[12,8,128,128]{3,2,1,0:T(8,128)}, f32[12,8,128]{2,1,0:T(8,128)}, f32[12,8]{1,0:T(8,128)}, bf16[12,1024]{1,0:T(8,128)(2,1)}) custom-call(bf16[4,16,1024]{2,1,0:T(8,128)(2,1)} %project.1.proj_ref, bf16[12,2048]{1,0:T(8,128)(2,1)} %resid_ref.5, f32[1,2048]{1,0:T(1,128)} %slice.4.gain_ref, bf16[8,2048]{1,0:T(8,128)(2,1)} %bitcast.12, ...), custom_call_target="tpu_custom_call" | custom-call | flops 6000000000 | bytes 12000000 | tf_op jit(solution)/shard_map/cell_update/pallas_call | solution.py:243
  43.3 0.0 copy-done.3
  43.3 0.1 copy.32
  43.4 0.0 copy-done.4
  43.4 0.1 copy.33
  43.5 0.7 fusion.table_ref
  44.2 0.0 copy-done.2
  44.2 0.6 broadcast_in_dim.28.gate_w_ref
  44.8 0.0 copy-start
  44.8 34.3 %branches.1 = bf16[12,2048]{1,0:T(8,128)(2,1)} custom-call(bf16[12,1024]{1,0:T(8,128)(2,1)} %get-tuple-element.8.gated_ref, bf16[12,2048]{1,0:T(8,128)(2,1)} %resid_ref.5, bf16[12,128]{1,0:T(8,128)(2,1)} %fusion.table_ref, f32[4,2048]{1,0:T(4,128)} %gains_ref.1, bf16[1,2048]{1,0:T(2,128)(2,1)} %broadcast_in_dim.28.gate_w_ref, bf16[1024,2048]{1,0:T(8,128)(2,1)} %mix_hbm.1, ...), custom_call_target="tpu_custom_call" | custom-call | flops 24999999488 | bytes 50000000 | tf_op jit(solution)/shard_map/branches/pallas_call | solution.py:372
  79.1 0.0 copy-done
  79.1 0.7 copy.34
  79.8 1.5 %copy.36 = bf16[12,2048]{1,0:T(8,128)(2,1)} copy(bf16[12,2048]{1,0:T(8,128)(2,1)} %branches.1) | data formatting | bytes 98304
Async XLA Ops:
  2.0 25.9 %copy-start.1 = (f32[12,8]{0,1:T(8,128)S(1)}, f32[12,8]{0,1:T(8,128)}, u32[]{:S(2)}) copy-start(f32[12,8]{0,1:T(8,128)} %param.35) | copy-start | bytes 1156
  28.6 14.7 %copy-start.3 = (s32[12,2]{0,1:T(2,128)S(1)}, s32[12,2]{0,1:T(2,128)}, u32[]{:S(2)}) copy-start(s32[12,2]{0,1:T(2,128)} %param.37) | copy-start | bytes 292
  28.6 14.8 %copy-start.4 = (bf16[12,2]{0,1:T(2,128)(2,1)S(1)}, bf16[12,2]{0,1:T(2,128)(2,1)}, u32[]{:S(2)}) copy-start(bf16[12,2]{0,1:T(2,128)(2,1)} %param.38) | copy-start | bytes 148
  28.6 15.6 %copy-start.2 = (bf16[2048]{0:T(1024)(128)(2,1)S(1)}, bf16[2048]{0:T(1024)(128)(2,1)}, u32[]{:S(2)}) copy-start(bf16[2048]{0:T(1024)(128)(2,1)} %param.45) | copy-start | bytes 12292
  44.8 34.3 %copy-start = (f32[12,8]{1,0:T(8,128)S(1)}, f32[12,8]{1,0:T(8,128)}, u32[]{:S(2)}) copy-start(f32[12,8]{1,0:T(8,128)} %get-tuple-element.19) | copy-start | bytes 1156

commit v3 on v2

--- a/solution.py
+++ b/solution.py
@@ -213,17 +213,19 @@
         q, k, kept = q3[s], k3[s], keep3[s]
         loading(s).wait()
         column = wv3[s].T
-        lane = lax.broadcasted_iota(jnp.int32, (size, heads), 1)
-        numer = jnp.zeros((size, heads), F32)
+        row = lax.broadcasted_iota(jnp.int32, (heads, size), 0)
+        numer = jnp.zeros((heads, size), F32)
+        q = q.astype(BF16)
         for h in range(heads):
             new = (
                 old[s, h] * kept[h : h + 1, :] + column[:, h : h + 1] * k[h : h + 1, :]
             )
             fresh[s, h] = new
-            read = jnp.sum(new * q[h : h + 1, :], axis=-1, keepdims=True)
-            numer = jnp.where(lane == h, read, numer)
+            high = new.astype(BF16)
+            low = (new - high.astype(F32)).astype(BF16)
+            numer = jnp.where(row == h, dot_t(q, high) + dot_t(q, low), numer)
         pltpu.make_async_copy(fresh.at[s], matrix_hbm.at[s], sem.at[s]).start()
-        numer3[s] = numer.T
+        numer3[s] = numer
         return carry
 
     lax.fori_loop(0, count, sequence, 0)

time: 81.6 us -> 77.3 us (0.947)
  Pallas kernels: 74.9 us -> 70.6 us
    pallas_call x1, Pallas kernels: 14.7 us -> 10.4 us  [cell_update(): pl.pallas_call(cell_kernel, out_shape=(jax.ShapeDtypeStruct(state.shape,...]
where the time goes in v3:
time: 77.3 us; the launch traced here: 77 us
  Pallas kernels  70.6 us (91%)
  local copies, waits for them, and re-layouts  4.99 us (6%)
    pallas_call x1, Pallas kernels, branches(): pl.pallas_call(functools.partial(branch_kernel, n), out_shape=jax.ShapeDt...  34.3 us
    pallas_call x1, Pallas kernels, project(): pl.pallas_call(functools.partial(project_kernel, n), out_shape=jax.ShapeD...  25.9 us
    pallas_call x1, Pallas kernels, cell_update(): pl.pallas_call(cell_kernel, out_shape=(jax.ShapeDtypeStruct(state.shape,...  10.4 us
    unnamed x14, local copies, waits for them, and re-layouts  2.93 us

profile of v3, /device:TPU:0, one launch (start us, length us, event | category | flops | bytes accessed | tf_op | source)
XLA Modules:
  0.0 77.0 jit_solution(12969912081362740058)
XLA Ops:
  0.6 1.4 %slice.4.gain_ref = f32[1,2048]{1,0:T(1,128)} slice(f32[4,2048]{1,0:T(4,128)} %gains_ref.1), slice={[0:1], [0:2048]} | slice | bytes 16384 | tf_op jit(solution)/shard_map/slice | solution.py:421
  2.0 0.0 copy-start.1
  2.0 25.9 %project.1.proj_ref = bf16[4,16,1024]{2,1,0:T(8,128)(2,1)} custom-call(bf16[12,2048]{1,0:T(8,128)(2,1)} %resid_ref.5, f32[1,2048]{1,0:T(1,128)} %slice.4.gain_ref, bf16[64,2048]{1,0:T(8,128)(2,1)} %bitcast.8, bf16[64,2048]{1,0:T(8,128)(2,1)} %bitcast.9, bf16[64,2048]{1,0:T(8,128)(2,1)} %bitcast.10, bf16[64,2048]{1,0:T(8,128)(2,1)} %bitcast.11), custom_call_target="tpu_custom_call" | custom-call | flops 20000000000 | bytes 40000000 | tf_op jit(solution)/shard_map/project/pallas_call | solution.py:150
  27.9 0.0 copy-done.1
  27.9 0.7 copy.31.max_ref
  28.6 0.0 copy-start.3
  28.6 0.0 copy-start.4
  28.6 0.0 copy-start.2
  28.6 10.4 %cell_update.1 = (f32[12,8,128,128]{3,2,1,0:T(8,128)}, f32[12,8,128]{2,1,0:T(8,128)}, f32[12,8]{1,0:T(8,128)}, bf16[12,1024]{1,0:T(8,128)(2,1)}) custom-call(bf16[4,16,1024]{2,1,0:T(8,128)(2,1)} %project.1.proj_ref, bf16[12,2048]{1,0:T(8,128)(2,1)} %resid_ref.5, f32[1,2048]{1,0:T(1,128)} %slice.4.gain_ref, bf16[8,2048]{1,0:T(8,128)(2,1)} %bitcast.12, ...), custom_call_target="tpu_custom_call" | custom-call | flops 6000000000 | bytes 12000000 | tf_op jit(solution)/shard_map/cell_update/pallas_call | solution.py:245
  39.0 0.0 copy-done.3
  39.0 0.1 copy.32
  39.1 0.0 copy-done.4
  39.1 0.1 copy.33
  39.2 0.7 fusion.table_ref
  39.9 0.0 copy-done.2
  39.9 0.6 broadcast_in_dim.28.gate_w_ref
  40.5 0.0 copy-start
  40.5 34.3 %branches.1 = bf16[12,2048]{1,0:T(8,128)(2,1)} custom-call(bf16[12,1024]{1,0:T(8,128)(2,1)} %get-tuple-element.8.gated_ref, bf16[12,2048]{1,0:T(8,128)(2,1)} %resid_ref.5, bf16[12,128]{1,0:T(8,128)(2,1)} %fusion.table_ref, f32[4,2048]{1,0:T(4,128)} %gains_ref.1, bf16[1,2048]{1,0:T(2,128)(2,1)} %broadcast_in_dim.28.gate_w_ref, bf16[1024,2048]{1,0:T(8,128)(2,1)} %mix_hbm.1, ...), custom_call_target="tpu_custom_call" | custom-call | flops 24999999488 | bytes 50000000 | tf_op jit(solution)/shard_map/branches/pallas_call | solution.py:374
  74.8 0.0 copy-done
  74.8 0.7 copy.34
  75.5 1.5 %copy.36 = bf16[12,2048]{1,0:T(8,128)(2,1)} copy(bf16[12,2048]{1,0:T(8,128)(2,1)} %branches.1) | data formatting | bytes 98304
Async XLA Ops:
  2.0 25.9 %copy-start.1 = (f32[12,8]{0,1:T(8,128)S(1)}, f32[12,8]{0,1:T(8,128)}, u32[]{:S(2)}) copy-start(f32[12,8]{0,1:T(8,128)} %param.35) | copy-start | bytes 1156
  28.6 10.4 %copy-start.3 = (s32[12,2]{0,1:T(2,128)S(1)}, s32[12,2]{0,1:T(2,128)}, u32[]{:S(2)}) copy-start(s32[12,2]{0,1:T(2,128)} %param.37) | copy-start | bytes 292
  28.6 10.5 %copy-start.4 = (bf16[12,2]{0,1:T(2,128)(2,1)S(1)}, bf16[12,2]{0,1:T(2,128)(2,1)}, u32[]{:S(2)}) copy-start(bf16[12,2]{0,1:T(2,128)(2,1)} %param.38) | copy-start | bytes 148
  28.6 11.3 %copy-start.2 = (bf16[2048]{0:T(1024)(128)(2,1)S(1)}, bf16[2048]{0:T(1024)(128)(2,1)}, u32[]{:S(2)}) copy-start(bf16[2048]{0:T(1024)(128)(2,1)} %param.45) | copy-start | bytes 12292
  40.5 34.3 %copy-start = (f32[12,8]{1,0:T(8,128)S(1)}, f32[12,8]{1,0:T(8,128)}, u32[]{:S(2)}) copy-start(f32[12,8]{1,0:T(8,128)} %get-tuple-element.19) | copy-start | bytes 1156
